TPU v7x, 32 devices: a whole 2x2x4 slice. The times are simulated.
32 devices in a mesh: fs: 8 (over z, y), tp: 4 (over x, core).
Axes of the slice: x: 2, y: 2, z: 4, core: 2. Of those that a mesh axis runs over, the one named last changes fastest.
Arguments:
- model_input: bfloat16 [16384, 2048], P('fs'), may hold values from -6 to 6
- value_cotan: bfloat16 [16384, 2048], P('fs', 'tp'), may hold values from -0.046875 to 0.046875
- mixer_cotan: bfloat16 [16384, 2048], P('fs'), may hold values from -0.046875 to 0.046875
- head_output: bfloat16 [16384, 2048], P('fs', 'tp'), may hold values from -6 to 6
- value_weight: float32 [2048, 2048], P('fs', 'tp'), may hold values from -0.125 to 0.125
- value_factor: bfloat16 [2048, 512], P('fs'), may hold values from -0.125 to 0.125
- value_first: float32 [512, 2048], P('fs', 'tp'), may hold values from -3 to 3
- value_second: float32 [512, 2048], P('fs', 'tp'), may hold values from 0.02 to 0.5
- output_weight: float32 [2048, 2048], P('fs', 'tp'), may hold values from -0.125 to 0.125
- output_factor: bfloat16 [2048, 512], P('fs'), may hold values from -0.125 to 0.125
- output_first: float32 [512, 2048], P('fs', 'tp'), may hold values from -3 to 3
- output_second: float32 [512, 2048], P('fs', 'tp'), may hold values from 0.02 to 0.5
Outputs:
- value_step: float32 [2048, 2048], P('fs', 'tp')
- value_updated: float32 [2048, 2048], P('fs', 'tp')
- value_first_new: float32 [512, 2048], P('fs', 'tp')
- value_second_new: float32 [512, 2048], P('fs', 'tp')
- value_copy: bfloat16 [2048, 2048], P(None, 'tp')
- output_step: float32 [2048, 2048], P('fs', 'tp')
- output_updated: float32 [2048, 2048], P('fs', 'tp')
- output_first_new: float32 [512, 2048], P('fs', 'tp')
- output_second_new: float32 [512, 2048], P('fs', 'tp')
- output_copy: bfloat16 [2048, 2048], P(None, 'tp')
All inputs are finite; a program needn't handle non-finite values.
Results may differ from a plain program's by a relative error of at most 0.0059.
Values may be sent and summed in bfloat16 or wider, within the bound.
A program may use at most 128 MiB of HBM per device.

v0:
```python
import jax
import jax.numpy as jnp
from jax import lax
from jax.sharding import PartitionSpec as P

D = 2048
HV = 2048


beta_first = 0.8
beta_second = 0.9
step_rate = 0.02
scale_floor = 0.25
tiny_eps = 1e-08


def low_rank(rows_in, cols_in, factor, first_moment, second_moment):
    token_dims = (((0,), (0,)), ((), ()))
    reduced = jnp.dot(
        rows_in,
        lax.all_gather(factor, "fs", axis=0, tiled=True),
        preferred_element_type=jnp.float32,
    )
    reduced_high = lax.optimization_barrier(reduced.astype(jnp.bfloat16))
    reduced_low = (reduced - reduced_high.astype(jnp.float32)).astype(jnp.bfloat16)
    high_part = lax.dot_general(
        reduced_high, cols_in, token_dims, preferred_element_type=jnp.float32
    )
    low_part = lax.dot_general(reduced_low, cols_in, token_dims, preferred_element_type=jnp.float32)
    projected = lax.psum_scatter(high_part + low_part, "fs", scatter_dimension=0, tiled=True)
    first_new = beta_first * first_moment + (1.0 - beta_first) * projected
    second_new = beta_second * second_moment + (1.0 - beta_second) * projected * projected
    direction = (first_new / (jnp.sqrt(second_new) + tiny_eps)).astype(jnp.bfloat16)
    expanded = jnp.dot(
        factor,
        lax.all_gather(direction, "fs", axis=0, tiled=True),
        preferred_element_type=jnp.float32,
    )
    return (expanded, first_new, second_new)


def local(
    model_input,
    value_cotan,
    mixer_cotan,
    head_output,
    value_weight,
    value_factor,
    value_first,
    value_second,
    output_weight,
    output_factor,
    output_first,
    output_second,
):
    value_exp, value_fnew, value_snew = low_rank(
        model_input, value_cotan, value_factor, value_first, value_second
    )
    output_exp, output_fnew, output_snew = low_rank(
        mixer_cotan, head_output, output_factor, output_first, output_second
    )
    value_sq, output_sq = lax.psum(
        (jnp.sum(value_exp * value_exp), jnp.sum(output_exp * output_exp)), ("fs", "tp")
    )
    value_step = step_rate / jnp.sqrt(value_sq / (D * HV) + scale_floor) * value_exp
    output_step = step_rate / jnp.sqrt(output_sq / (D * HV) + scale_floor) * output_exp
    value_updated = value_weight - value_step
    output_updated = output_weight - output_step
    value_copy, output_copy = (
        lax.all_gather(value_updated.astype(jnp.bfloat16), "fs", axis=0, tiled=True),
        lax.all_gather(output_updated.astype(jnp.bfloat16), "fs", axis=0, tiled=True),
    )
    return (
        value_step,
        value_updated,
        value_fnew,
        value_snew,
        value_copy,
        output_step,
        output_updated,
        output_fnew,
        output_snew,
        output_copy,
    )


def solution(mesh):
    placed = (
        P("fs", None),
        P("fs", "tp"),
        P("fs", None),
        P("fs", "tp"),
        P("fs", "tp"),
        P("fs", None),
        P("fs", "tp"),
        P("fs", "tp"),
        P("fs", "tp"),
        P("fs", None),
        P("fs", "tp"),
        P("fs", "tp"),
    )
    return jax.shard_map(
        local,
        mesh=mesh,
        in_specs=placed,
        out_specs=(
            P("fs", "tp"),
            P("fs", "tp"),
            P("fs", "tp"),
            P("fs", "tp"),
            P(None, "tp"),
            P("fs", "tp"),
            P("fs", "tp"),
            P("fs", "tp"),
            P("fs", "tp"),
            P(None, "tp"),
        ),
        check_vma=False,
    )
```

profile of v0, /device:TPU:17, one launch (start us, length us, event | category | flops | bytes accessed | tf_op | source)
XLA Modules:
  0.0 429.9 jit_solution(7380048954064010271)
XLA Ops:
  7.2 0.0 copy-start
  7.2 0.0 all-gather.9.cloned.1.call-start
  7.2 0.7 all-gather.9.cloned.1.call-update
  7.9 0.0 all-gather.5.cloned.1.call-start
  8.0 0.7 all-gather.5.cloned.1.call-update
  8.7 0.0 reduce-scatter.5.cloned.1.call-start
  8.7 50.3 %all-gather.9.cloned.1.call-done = bf16[2048,512]{1,0:T(8,128)(2,1)} async-done(((bf16[256,512]{1,0:T(8,128)(2,1)}), bf16[2048,512]{1,0:T(8,128)(2,1)}) %all-gather.9.cloned.1.call-update) | async-done | bytes 2097168 | tf_op jit(solution)/shard_map/all_gather | solution.py:21
  59.0 7.5 %fusion.11 = (bf16[2048,512]{1,0:T(8,128)(2,1)S(1)}, f32[2048,512]{1,0:T(8,128)S(1)}) fusion(bf16[2048,2048]{1,0:T(8,128)(2,1)} %param.14, bf16[2048,512]{1,0:T(8,128)(2,1)} %all-gather.9.cloned.1.call-done), kind=kOutput, calls=%fused_computation.21 | convolution fusion | flops 4296015872 | bytes 16777216 | tf_op jit(solution)/shard_map/dot_general | solution.py:19
  66.6 0.0 copy-done
  66.6 1.3 fusion.13
  67.9 2.4 fusion.2
  70.3 0.0 reduce-scatter.5.cloned.1.call-update
  70.3 0.0 reduce-scatter.3.cloned.1.call-start
  70.3 38.5 %all-gather.5.cloned.1.call-done = bf16[2048,512]{1,0:T(8,128)(2,1)} async-done(((bf16[256,512]{1,0:T(8,128)(2,1)}), bf16[2048,512]{1,0:T(8,128)(2,1)}) %all-gather.5.cloned.1.call-update) | async-done | bytes 2097168 | tf_op jit(solution)/shard_map/all_gather | solution.py:21
  108.8 0.0 copy-start.1
  108.8 7.7 %fusion.10 = (bf16[2048,512]{1,0:T(8,128)(2,1)S(1)}, f32[2048,512]{1,0:T(8,128)S(1)}) fusion(bf16[2048,2048]{1,0:T(8,128)(2,1)} %param.12, bf16[2048,512]{1,0:T(8,128)(2,1)} %all-gather.5.cloned.1.call-done), kind=kOutput, calls=%fused_computation.20 | convolution fusion | flops 4296015872 | bytes 16777216 | tf_op jit(solution)/shard_map/dot_general | solution.py:19
  116.5 0.0 copy-done.1
  116.5 1.3 fusion.12
  117.8 0.0 copy-start.6
  117.8 2.3 fusion.3
  120.1 0.0 copy-start.7
  120.1 0.0 copy-start.8
  120.1 0.0 copy-start.4
  120.1 0.0 reduce-scatter.3.cloned.1.call-update
  120.1 0.0 copy-start.9
  120.1 0.0 all-gather.11.cloned.1.call-start
  120.2 0.0 copy-done.6
  120.2 1.0 copy.23
  121.2 0.0 copy-start.5
  121.2 52.6 %reduce-scatter.5.cloned.1.call-done = f32[64,512]{1,0:T(8,128)} async-done(((f32[512,512]{1,0:T(8,128)}), f32[64,512]{1,0:T(8,128)}) %reduce-scatter.5.cloned.1.call-update) | async-done | bytes 131088 | tf_op jit(solution)/shard_map/reduce_scatter | solution.py:30
  173.8 0.0 copy-done.7
  173.8 0.0 copy-done.8
  173.8 1.7 divide_convert_fusion
  175.4 23.4 %all_gather.22 = bf16[512,512]{1,0:T(8,128)(2,1)S(1)} all-gather(bf16[64,512]{1,0:T(8,128)(2,1)S(1)} %get-tuple-element.28), channel_id=1, replica_groups=mesh['fs'=8,'tp'=4] {'fs'}, dimensions={0}, use_global_device_ids=true | all-gather | bytes 589824 | tf_op jit(solution)/shard_map/all_gather | solution.py:36
  198.9 0.0 copy-done.4
  198.9 1.0 multiply_reduce_fusion
  199.8 41.3 %reduce-scatter.3.cloned.1.call-done = f32[64,512]{1,0:T(8,128)} async-done(((f32[512,512]{1,0:T(8,128)}), f32[64,512]{1,0:T(8,128)}) %reduce-scatter.3.cloned.1.call-update) | async-done | bytes 131088 | tf_op jit(solution)/shard_map/reduce_scatter | solution.py:30
  241.1 0.0 copy-done.9
  241.1 1.7 divide_convert_fusion.1
  242.8 22.5 %all_gather.19 = bf16[512,512]{1,0:T(8,128)(2,1)S(1)} all-gather(bf16[64,512]{1,0:T(8,128)(2,1)S(1)} %get-tuple-element.31), channel_id=1, replica_groups=mesh['fs'=8,'tp'=4] {'fs'}, dimensions={0}, use_global_device_ids=true | all-gather | bytes 589824 | tf_op jit(solution)/shard_map/all_gather | solution.py:36
  265.3 0.0 copy-done.5
  265.3 1.0 multiply_reduce_fusion.1
  266.3 49.5 %all-reduce = (f32[]{:T(128)}, f32[]{:T(128)}) all-reduce(f32[]{:T(128)} %get-tuple-element.36, f32[]{:T(128)} %get-tuple-element.40), channel_id=1, replica_groups=mesh['fs'=8,'tp'=4] {'fs','tp'}, use_global_device_ids=true, to_apply=%region_2.0 | all-reduce | flops 2 | bytes 16 | tf_op jit(solution)/shard_map/psum | solution.py:62
  316.5 2.2 fusion.6
  318.7 0.0 all-gather.11.cloned.1.call-update
  318.7 0.0 all-gather.7.cloned.1.call-start
  318.8 2.0 copy.22
  320.8 0.0 copy-start.2
  321.6 2.2 fusion.7
  323.8 0.0 copy-start.3
  323.8 0.0 all-gather.7.cloned.1.call-update
  323.8 2.1 copy.27
  325.9 0.0 copy-done.2
  325.9 1.0 copy.28
  326.9 2.1 copy.24
  328.9 0.0 copy-done.3
  328.9 1.0 copy.25
  329.9 38.7 %all-gather.11.cloned.1.call-done = bf16[2048,512]{0,1:T(8,128)(2,1)} async-done(((bf16[256,512]{0,1:T(8,128)(2,1)}), bf16[2048,512]{0,1:T(8,128)(2,1)}) %all-gather.11.cloned.1.call-update) | async-done | bytes 2097168 | tf_op jit(solution)/shard_map/all_gather | solution.py:71
  368.7 3.9 copy.29
  372.6 46.5 %all-gather.7.cloned.1.call-done = bf16[2048,512]{0,1:T(8,128)(2,1)} async-done(((bf16[256,512]{0,1:T(8,128)(2,1)}), bf16[2048,512]{0,1:T(8,128)(2,1)}) %all-gather.7.cloned.1.call-update) | async-done | bytes 2097168 | tf_op jit(solution)/shard_map/all_gather | solution.py:70
  419.1 3.9 copy.26
Async XLA Ops:
  7.2 59.4 %copy-start = (bf16[2048,512]{1,0:T(8,128)(2,1)S(1)}, bf16[2048,512]{1,0:T(8,128)(2,1)}, u32[]{:S(2)}) copy-start(bf16[2048,512]{1,0:T(8,128)(2,1)} %param.15) | copy-start | bytes 6291460
  7.2 51.9 %all-gather.9.cloned.1.call-start = ((), (), s32[]{:S(2)}) async-start(), calls=%async_computation.5 | async-start | bytes 2359296 | tf_op jit(solution)/shard_map/all_gather | solution.py:21
  7.9 100.9 %all-gather.5.cloned.1.call-start = ((), (), s32[]{:S(2)}) async-start(), calls=%async_computation.2 | async-start | bytes 2359296 | tf_op jit(solution)/shard_map/all_gather | solution.py:21
  8.7 165.1 %reduce-scatter.5.cloned.1.call-start = ((), (), s32[]{:S(2)}) async-start(), calls=%async_computation.6 | async-start | bytes 1179648 | tf_op jit(solution)/shard_map/reduce_scatter | solution.py:30
  70.3 170.8 %reduce-scatter.3.cloned.1.call-start = ((), (), s32[]{:S(2)}) async-start(), calls=%async_computation.3 | async-start | bytes 1179648 | tf_op jit(solution)/shard_map/reduce_scatter | solution.py:30
  108.8 7.7 %copy-start.1 = (bf16[2048,512]{1,0:T(8,128)(2,1)S(1)}, bf16[2048,512]{1,0:T(8,128)(2,1)}, u32[]{:S(2)}) copy-start(bf16[2048,512]{1,0:T(8,128)(2,1)} %param.13) | copy-start | bytes 6291460
  117.8 2.4 copy-start.6
  120.1 53.7 %copy-start.7 = (f32[64,512]{1,0:T(8,128)S(1)}, f32[64,512]{1,0:T(8,128)}, u32[]{:S(2)}) copy-start(f32[64,512]{1,0:T(8,128)} %param.23) | copy-start | bytes 393220
  120.1 53.7 %copy-start.8 = (f32[64,512]{1,0:T(8,128)S(1)}, f32[64,512]{1,0:T(8,128)}, u32[]{:S(2)}) copy-start(f32[64,512]{1,0:T(8,128)} %param.22) | copy-start | bytes 393220
  120.1 78.8 %copy-start.4 = (bf16[256,512]{1,0:T(8,128)(2,1)S(1)}, bf16[256,512]{1,0:T(8,128)(2,1)}, u32[]{:S(2)}) copy-start(bf16[256,512]{1,0:T(8,128)(2,1)} %param.21) | copy-start | bytes 786436
  120.1 121.0 %copy-start.9 = (f32[64,512]{1,0:T(8,128)S(1)}, f32[64,512]{1,0:T(8,128)}, u32[]{:S(2)}) copy-start(f32[64,512]{1,0:T(8,128)} %param.19) | copy-start | bytes 393220
  120.1 248.6 %all-gather.11.cloned.1.call-start = ((), (), s32[]{:S(2)}) async-start(), calls=%async_computation.7 | async-start | bytes 2359296 | tf_op jit(solution)/shard_map/all_gather | solution.py:71
  121.2 144.2 %copy-start.5 = (bf16[256,512]{1,0:T(8,128)(2,1)S(1)}, bf16[256,512]{1,0:T(8,128)(2,1)}, u32[]{:S(2)}) copy-start(bf16[256,512]{1,0:T(8,128)(2,1)} %param.17) | copy-start | bytes 786436
  318.7 100.4 %all-gather.7.cloned.1.call-start = ((), (), s32[]{:S(2)}) async-start(), calls=%async_computation.4 | async-start | bytes 2359296 | tf_op jit(solution)/shard_map/all_gather | solution.py:70
  320.8 5.1 %copy-start.2 = (f32[256,512]{0,1:T(8,128)S(1)}, f32[256,512]{0,1:T(8,128)}, u32[]{:S(2)}) copy-start(f32[256,512]{0,1:T(8,128)} %get-tuple-element.23) | copy-start | bytes 1572868
  323.8 5.2 %copy-start.3 = (f32[256,512]{0,1:T(8,128)S(1)}, f32[256,512]{0,1:T(8,128)}, u32[]{:S(2)}) copy-start(f32[256,512]{0,1:T(8,128)} %get-tuple-element.26) | copy-start | bytes 1572868
Sparse Core Ops, SparseCore 0:
  10.1 48.8 all-gather.8
  61.2 47.6 all-gather.4
  112.8 60.9 reduce-scatter.4
  177.6 63.4 reduce-scatter.2
  318.8 49.7 all-gather.10
  370.6 48.5 all-gather.6
where the time goes:
time: 434 us; the launch traced here: 430 us
  waiting for transfers between devices  269 us (62%)
  blocking collectives  95.4 us (22%)
  matrix products  24.3 us (6%)
  local copies, waits for them, and re-layouts  17 us (4%)
  between operations  15.6 us (4%)
  other arithmetic  7.82 us (2%)
    reduce_scatter x2, waiting for transfers between devices, low_rank(): lax.psum_scatter(high_part + low_part, 'fs', scatter_dimension=0, tiled=T...  93.9 us
    all_gather x2, waiting for transfers between devices, low_rank(): lax.all_gather(factor, 'fs', axis=0, tiled=True)  88.8 us
    psum x1, blocking collectives, local(): lax.psum((jnp.sum(value_exp * value_exp), jnp.sum(output_exp * output_exp...  49.5 us
    all_gather x1, waiting for transfers between devices, local(): lax.all_gather(value_updated.astype(jnp.bfloat16), 'fs', axis=0, tiled=True)  46.5 us
    all_gather x2, blocking collectives, low_rank(): lax.all_gather(direction, 'fs', axis=0, tiled=True)  45.9 us
    all_gather x1, waiting for transfers between devices, local(): lax.all_gather(output_updated.astype(jnp.bfloat16), 'fs', axis=0, tiled=T...  38.7 us
    unnamed x28, local copies, waits for them, and re-layouts  17 us
    dot_general x2, matrix products, low_rank(): jnp.dot(rows_in, lax.all_gather(factor, 'fs', axis=0, tiled=True), prefer...  15.2 us
  transfers between devices with their start and end apart: 6, of which 6 were waited for; matrix products, arithmetic and copies ran while one was open for 9% of the time, Pallas kernels for 0%

commit v1 on v0

v1 whole, which is shorter than its diff:
```python
import functools

import jax
import jax.numpy as jnp
from jax import lax
from jax.experimental import pallas as pl
from jax.experimental.pallas import tpu as pltpu
from jax.sharding import PartitionSpec as P

beta_first = 0.8
beta_second = 0.9
step_rate = 0.02
scale_floor = 0.25
tiny_eps = 1e-08

MESH = pl.DeviceIdType.MESH
F32 = jnp.float32
BF16 = jnp.bfloat16
VMEM_LIMIT = 67_000_000
W_HOOK = (0, 1, 2)


def kernel(
    n,
    ntp,
    rows_v, cols_v, rows_o, cols_o,
    fac_ref, w_v, w_o, first_v, first_o, second_v, second_o,
    step_v, upd_v, fnew_v, snew_v, copy_v,
    step_o, upd_o, fnew_o, snew_o, copy_o,
    rows, cols, fg, wg, acc, e_buf, pf, pg, send_a, recv_a, send_b, recv_b,
    dirg, ss, ssg,
    sem_rows, sem_cols,
    fs_z, fr_z, fs_y, fr_y, fs_c, fr_c,
    ws_z, wr_z, ws_y, wr_y,
    as_, ar, bs, br,
    ds_z, dr_z, ds_y, dr_y,
    ps, pr,
):
    nz = n // 2
    me = lax.axis_index("fs")
    tp = lax.axis_index("tp")
    z, y = me // 2, lax.rem(me, 2)
    ybar = 1 - y
    mate = 2 * z + ybar
    core = lax.rem(tp, 2)
    other = 1 - core
    twin = tp + 1 - 2 * core
    T, D = rows_v.shape
    C = cols_v.shape[1]
    R, K = fac_ref.shape[1:]
    k = first_v.shape[0]
    TC = 512

    def zup(d):
        return lax.rem(z + d, nz)

    def zdn(d):
        return lax.rem(z + nz - d, nz)

    def rcopy(src, dst, ssem, rsem, dev):
        return pltpu.make_async_remote_copy(
            src_ref=src, dst_ref=dst, send_sem=ssem, recv_sem=rsem,
            device_id=dev, device_id_type=MESH,
        )

    def fsdev(i):
        return (i, tp)

    loads = []
    for m, (r, c) in enumerate(((rows_v, cols_v), (rows_o, cols_o))):
        loads.append(pltpu.make_async_copy(r, rows.at[m], sem_rows.at[m]))
        loads.append(pltpu.make_async_copy(c, cols.at[m], sem_cols.at[m]))
    for i in (0, 2, 1, 3):
        loads[i].start()

    barrier = pltpu.get_barrier_semaphore()
    for d in range(1, nz):
        pl.semaphore_signal(
            barrier, inc=1, device_id=fsdev(2 * zup(d) + y), device_id_type=MESH
        )
    pl.semaphore_signal(barrier, inc=1, device_id=fsdev(mate), device_id_type=MESH)
    for q in range(1, ntp):
        pl.semaphore_signal(
            barrier, inc=1, device_id=(me, lax.rem(tp + q, ntp)), device_id_type=MESH
        )
    pl.semaphore_wait(barrier, nz - 1 + 1 + ntp - 1)

    pend = []

    for d in list(range(1, nz)):
        c = rcopy(fac_ref.at[core], fg.at[core, me], fs_z.at[d], fr_z.at[d], fsdev(2 * zup(d) + y))
        c.start()
        pend.append(c)
    c = rcopy(fac_ref.at[core], fg.at[core, me], fs_y.at[0], fr_y.at[0], fsdev(mate))
    c.start()
    pend.append(c)
    for m in range(2):
        fg[m, me] = fac_ref[m]
    wg[me, 0] = w_v[...].astype(BF16)
    wg[me, 1] = w_o[...].astype(BF16)

    def w_send(d):
        if d == 0:
            c = rcopy(wg.at[me], wg.at[me], ws_y.at[0], wr_y.at[0], fsdev(mate))
        else:
            c = rcopy(wg.at[me], wg.at[me], ws_z.at[d], wr_z.at[d], fsdev(2 * zup(d) + y))
        c.start()
        pend.append(c)

    def w_forward(d):
        i = 2 * zdn(d) + y
        rcopy(wg.at[i], wg.at[i], ws_z.at[d], wr_z.at[d], fsdev(mate)).wait_recv()
        c = rcopy(wg.at[i], wg.at[i], ws_y.at[d], wr_y.at[d], fsdev(mate))
        c.start()
        pend.append(c)

    def w_finish(d):
        i = 2 * zdn(d) + ybar
        rcopy(wg.at[i], wg.at[i], ws_y.at[d], wr_y.at[d], fsdev(mate)).wait_recv()

    def to_twin(i, q):
        c = rcopy(fg.at[core, i], fg.at[core, i], fs_c.at[q], fr_c.at[q], (me, twin))
        c.start()
        pend.append(c)

    def f_recv(sems, d, i):
        rcopy(fg.at[core, i], fg.at[core, i], fs_z.at[0], sems.at[d], fsdev(mate)).wait_recv()

    def f_recv_twin(i, q):
        rcopy(fg.at[other, i], fg.at[other, i], fs_c.at[0], fr_c.at[q], (me, twin)).wait_recv()

    def accumulate(m, d):
        p = zdn(d)
        pair = jnp.concatenate([fg[m, 2 * p], fg[m, 2 * p + 1]], axis=0)
        pair_t = pair.T

        @pl.loop(0, T // TC)
        def _(t):
            at = pl.ds(pl.multiple_of(t * TC, TC), TC)
            lhs = rows[m, at, pl.ds(pl.multiple_of(p * 2 * R, 2 * R), 2 * R)]
            prod = lax.dot_general(
                pair_t, lhs, (((1,), (1,)), ((), ())), preferred_element_type=F32
            )
            if d == 0:
                acc[m, :, at] = prod
            else:
                acc[m, :, at] += prod

    for d in range(nz):
        if d > 0:
            i = 2 * zdn(d) + y
            f_recv(fr_z, d, i)
            c = rcopy(fg.at[core, i], fg.at[core, i], fs_y.at[d], fr_y.at[d], fsdev(mate))
            c.start()
            pend.append(c)
            to_twin(i, 2 * d)
        i = 2 * zdn(d) + ybar
        f_recv(fr_y, d, i)
        to_twin(i, 2 * d + 1)
        if d == 0:
            for h in range(nz):
                if h < len(W_HOOK) and W_HOOK[h] == 0 or h >= len(W_HOOK):
                    w_send(h)
            loads[0].wait()
            loads[2].wait()
        accumulate(core, d)
        if d > 0:
            f_recv_twin(2 * zdn(d) + y, 2 * d)
        f_recv_twin(i, 2 * d + 1)
        accumulate(other, d)
    loads[1].wait()
    loads[3].wait()

    def hook(v):
        for h in range(min(nz, len(W_HOOK))):
            if W_HOOK[h] == v:
                w_send(h)

    def partial_products(m):
        @pl.loop(0, T // TC)
        def _(t):
            at = pl.ds(pl.multiple_of(t * TC, TC), TC)
            red = acc[m, :, at].astype(BF16)
            prod = jnp.dot(red, cols[m, at, :], preferred_element_type=F32)
            prod = prod.reshape(n, k, C)

            @pl.when(t == 0)
            def _():
                pf[m] = prod

            @pl.when(t > 0)
            def _():
                pf[m] += prod

        for h in range(nz):
            send_a[m, h] = pf[m, 2 * zup(h) + ybar].astype(BF16)
        for h in [*range(1, nz), 0]:
            c = rcopy(
                send_a.at[m, h], recv_a.at[m, h], as_.at[m, h], ar.at[m, h], fsdev(mate)
            )
            c.start()
            pend.append(c)

    def middle(m):
        for h in [*range(1, nz), 0]:
            rcopy(
                send_a.at[m, h], recv_a.at[m, h], as_.at[m, h], ar.at[m, h], fsdev(mate)
            ).wait_recv()
            tot = pf[m, 2 * zup(h) + y] + recv_a[m, h].astype(F32)
            if h == 0:
                pg[m] = tot
            else:
                send_b[m, h] = tot.astype(BF16)
                c = rcopy(
                    send_b.at[m, h], recv_b.at[m, h], bs.at[m, h], br.at[m, h],
                    fsdev(2 * zup(h) + y),
                )
                c.start()
                pend.append(c)

    def moments(m, first, second, fnew, snew):
        tot = pg[m]
        for h in range(1, nz):
            rcopy(
                send_b.at[m, h], recv_b.at[m, h], bs.at[m, h], br.at[m, h], fsdev(mate)
            ).wait_recv()
            tot = tot + recv_b[m, h].astype(F32)
        f = beta_first * first[...] + (1.0 - beta_first) * tot
        s = beta_second * second[...] + (1.0 - beta_second) * tot * tot
        fnew[...] = f
        snew[...] = s
        dirg[m, me] = (f / (jnp.sqrt(s) + tiny_eps)).astype(BF16)
        for h in range(1, nz):
            c = rcopy(
                dirg.at[m, me], dirg.at[m, me], ds_z.at[m, h], dr_z.at[m, h],
                fsdev(2 * zup(h) + y),
            )
            c.start()
            pend.append(c)
        c = rcopy(dirg.at[m, me], dirg.at[m, me], ds_y.at[m, 0], dr_y.at[m, 0], fsdev(mate))
        c.start()
        pend.append(c)

    def dir_forward(m):
        for h in range(1, nz):
            i = 2 * zdn(h) + y
            rcopy(
                dirg.at[m, i], dirg.at[m, i], ds_z.at[m, h], dr_z.at[m, h], fsdev(mate)
            ).wait_recv()
            c = rcopy(dirg.at[m, i], dirg.at[m, i], ds_y.at[m, h], dr_y.at[m, h], fsdev(mate))
            c.start()
            pend.append(c)

    def expand(m):
        for h in range(nz):
            i = 2 * zdn(h) + ybar
            rcopy(
                dirg.at[m, i], dirg.at[m, i], ds_y.at[m, h], dr_y.at[m, h], fsdev(mate)
            ).wait_recv()
        ss[m] = jnp.zeros(ss.shape[1:], F32)

        @pl.loop(0, nz)
        def _(b):
            lhs = fg[m, pl.ds(2 * b, 2)].reshape(2 * R, K)
            ex = jnp.dot(lhs, dirg[m].reshape(n * k, C), preferred_element_type=F32)
            e_buf[m, pl.ds(2 * b, 2)] = ex.reshape(2, R, C)
            ss[m] += jnp.sum((ex * ex).reshape(2 * R // 8, 8, C), axis=0)

        for q in range(1, ntp):
            c = rcopy(
                ss.at[m], ssg.at[m, q], ps.at[m, q], pr.at[m, q],
                (me, lax.rem(tp + q, ntp)),
            )
            c.start()
            pend.append(c)

    def finish(m, weight, step, upd, copy):
        tot = ss[m]
        for q in range(1, ntp):
            rcopy(ss.at[m], ssg.at[m, q], ps.at[m, q], pr.at[m, q], (me, twin)).wait_recv()
            tot = tot + ssg[m, q]
        mean = jnp.sum(tot, keepdims=True) / (n * R * C * ntp)
        scale = step_rate / jnp.sqrt(mean + scale_floor)
        s = scale * e_buf[m, me]
        step[...] = s
        upd[...] = weight[...] - s

        @pl.loop(0, n)
        def _(b):
            at = pl.ds(pl.multiple_of(b * R, R), R)
            copy[at, :] = (wg[b, m].astype(F32) - scale * e_buf[m, b]).astype(BF16)

    partial_products(0)
    partial_products(1)
    middle(0)
    middle(1)
    hook(1)
    moments(0, first_v, second_v, fnew_v, snew_v)
    moments(1, first_o, second_o, fnew_o, snew_o)
    hook(2)
    dir_forward(0)
    dir_forward(1)
    expand(0)
    expand(1)
    for h in range(1, nz):
        w_forward(h)
    for h in range(nz):
        w_finish(h)
    finish(0, w_v, step_v, upd_v, copy_v)
    finish(1, w_o, step_o, upd_o, copy_o)
    for c in pend:
        c.wait_send()


def local(
    n, ntp,
    model_input, value_cotan, mixer_cotan, head_output,
    value_weight, value_factor, value_first, value_second,
    output_weight, output_factor, output_first, output_second,
):
    T, D = model_input.shape
    C = value_cotan.shape[1]
    R, K = value_factor.shape
    k = value_first.shape[0]
    nz = n // 2
    vm = pl.BlockSpec(memory_space=pltpu.VMEM)
    hbm = pl.BlockSpec(memory_space=pl.ANY)
    wide = jax.ShapeDtypeStruct((R, C), F32)
    mom = jax.ShapeDtypeStruct((k, C), F32)
    full = jax.ShapeDtypeStruct((n * R, C), BF16)
    dma = pltpu.SemaphoreType.DMA
    return pl.pallas_call(
        functools.partial(kernel, n, ntp),
        out_shape=(wide, wide, mom, mom, full) * 2,
        in_specs=[hbm] * 4 + [vm] * 7,
        out_specs=(vm,) * 10,
        scratch_shapes=[
            pltpu.VMEM((2, T, D), BF16),
            pltpu.VMEM((2, T, C), BF16),
            pltpu.VMEM((2, n, R, K), BF16),
            pltpu.VMEM((n, 2, R, C), BF16),
            pltpu.VMEM((2, K, T), F32),
            pltpu.VMEM((2, n, R, C), F32),
            pltpu.VMEM((2, n, k, C), F32),
            pltpu.VMEM((2, k, C), F32),
            pltpu.VMEM((2, nz, k, C), BF16),
            pltpu.VMEM((2, nz, k, C), BF16),
            pltpu.VMEM((2, nz, k, C), BF16),
            pltpu.VMEM((2, nz, k, C), BF16),
            pltpu.VMEM((2, n, k, C), BF16),
            pltpu.VMEM((2, 8, C), F32),
            pltpu.VMEM((2, ntp, 8, C), F32),
            dma((2,)), dma((2,)),
            dma((nz,)), dma((nz,)), dma((nz,)), dma((nz,)), dma((n,)), dma((n,)),
            dma((nz,)), dma((nz,)), dma((nz,)), dma((nz,)),
            dma((2, nz)), dma((2, nz)), dma((2, nz)), dma((2, nz)),
            dma((2, nz)), dma((2, nz)), dma((2, nz)), dma((2, nz)),
            dma((2, ntp)), dma((2, ntp)),
        ],
        compiler_params=pltpu.CompilerParams(
            collective_id=0, has_side_effects=True, vmem_limit_bytes=VMEM_LIMIT
        ),
    )(
        model_input, value_cotan, mixer_cotan, head_output,
        jnp.stack([value_factor, output_factor]),
        value_weight, output_weight,
        value_first, output_first, value_second, output_second,
    )


def solution(mesh):
    rows, both, full = P("fs", None), P("fs", "tp"), P(None, "tp")
    return jax.shard_map(
        functools.partial(local, mesh.shape["fs"], mesh.shape["tp"]),
        mesh=mesh,
        in_specs=(rows, both, rows, both) + (both, rows, both, both) * 2,
        out_specs=(both, both, both, both, full) * 2,
        check_vma=False,
    )
```

time: 434 us -> 178 us (0.41)
  the two profiles are of different devices: /device:TPU:17 before, /device:TPU:0 now
where the time goes in v1:
time: 178 us
  Pallas kernels  164 us (92%)
  local copies, waits for them, and re-layouts  11.7 us (7%)
  other arithmetic  1.87 us (1%)
    pallas_call x1, Pallas kernels, local(): pl.pallas_call(functools.partial(kernel, n, ntp), out_shape=(wide, wide,...  164 us
    unnamed x24, local copies, waits for them, and re-layouts  11.7 us

profile of v1, /device:TPU:0, one launch (start us, length us, event | category | flops | bytes accessed | tf_op | source)
XLA Modules:
  0.0 178.1 jit_solution(8097738902572925588)
XLA Ops:
  0.6 1.9 %pad_maximum_fusion.fac_ref = bf16[2,256,512]{2,1,0:T(8,128)(2,1)} fusion(bf16[1,256,512]{2,1,0:T(8,128)(2,1)} %bitcast.2, bf16[1,256,512]{2,1,0:T(8,128)(2,1)} %bitcast.3), kind=kLoop, calls=%fused_computation | loop fusion | flops 262144 | bytes 1048576 | tf_op jit(solution)/shard_map/stack | solution.py:365
  2.5 163.9 %shard_map.195 = (f32[256,512]{1,0:T(8,128)}, f32[256,512]{1,0:T(8,128)}, f32[64,512]{1,0:T(8,128)}, f32[64,512]{1,0:T(8,128)}, bf16[2048,512]{1,0:T(8,128)(2,1)...) custom-call(bf16[2048,2048]{1,0:T(8,128)(2,1)} %rows_v.1, ...), custom_call_target="tpu_custom_call" | custom-call | tf_op jit(solution)/shard_map/pallas_call | solution.py:332
  166.4 0.0 copy-start.6
  166.4 0.0 copy-start.1
  166.4 2.0 %copy.32 = f32[256,512]{1,0:T(8,128)} copy(f32[256,512]{1,0:T(8,128)} %get-tuple-element.20) | data formatting | bytes 1048576
  168.4 1.9 %copy.33 = f32[256,512]{1,0:T(8,128)} copy(f32[256,512]{1,0:T(8,128)} %get-tuple-element.21) | data formatting | bytes 1048576
  170.3 1.6 copy.34
  171.9 0.0 copy-done.6
  171.9 0.7 copy.35
  172.5 0.0 copy-done.1
  172.5 0.0 copy-start.3
  172.5 0.0 copy-start.2
  172.5 0.0 copy-start.5
  172.5 1.3 copy.36
  173.9 0.0 copy-done.3
  173.9 0.0 copy-start.4
  173.9 0.0 copy-start
  173.9 0.8 copy.37
  174.7 0.0 copy-done.2
  174.7 0.8 copy.38
  175.5 0.0 copy-done.5
  175.5 0.7 copy.39
  176.2 0.0 copy-done.4
  176.2 0.7 copy.40
  176.8 0.0 copy-done
  176.8 1.3 copy.41
Async XLA Ops:
  166.4 5.5 %copy-start.6 = (f32[64,512]{1,0:T(8,128)S(1)}, f32[64,512]{1,0:T(8,128)}, u32[]{:S(2)}) copy-start(f32[64,512]{1,0:T(8,128)} %get-tuple-element.23) | copy-start | bytes 393220
  166.4 6.1 %copy-start.1 = (bf16[2048,512]{1,0:T(8,128)(2,1)S(1)}, bf16[2048,512]{1,0:T(8,128)(2,1)}, u32[]{:S(2)}) copy-start(bf16[2048,512]{1,0:T(8,128)(2,1)} %get-tuple-element.24) | copy-start | bytes 6291460
  172.5 1.4 copy-start.3
  172.5 2.2 %copy-start.2 = (f32[256,512]{1,0:T(8,128)S(1)}, f32[256,512]{1,0:T(8,128)}, u32[]{:S(2)}) copy-start(f32[256,512]{1,0:T(8,128)} %get-tuple-element.26) | copy-start | bytes 1572868
  172.5 3.0 %copy-start.5 = (f32[64,512]{1,0:T(8,128)S(1)}, f32[64,512]{1,0:T(8,128)}, u32[]{:S(2)}) copy-start(f32[64,512]{1,0:T(8,128)} %get-tuple-element.27) | copy-start | bytes 393220
  173.9 2.3 %copy-start.4 = (f32[64,512]{1,0:T(8,128)S(1)}, f32[64,512]{1,0:T(8,128)}, u32[]{:S(2)}) copy-start(f32[64,512]{1,0:T(8,128)} %get-tuple-element.28) | copy-start | bytes 393220
  173.9 2.9 %copy-start = (bf16[2048,512]{1,0:T(8,128)(2,1)S(1)}, bf16[2048,512]{1,0:T(8,128)(2,1)}, u32[]{:S(2)}) copy-start(bf16[2048,512]{1,0:T(8,128)(2,1)} %get-tuple-element.29) | copy-start | bytes 6291460

commit v2 on v1

--- a/solution.py
+++ b/solution.py
@@ -17,7 +17,7 @@
 F32 = jnp.float32
 BF16 = jnp.bfloat16
 VMEM_LIMIT = 67_000_000
-W_HOOK = (0, 1, 2)
+PLAN = (((1, 0), (1, 1), (1, 3), (1, 2)), ((2, 3),), ((2, 2),), (), (), (), ((2, 1),))
 
 
 def kernel(
@@ -30,7 +30,7 @@
     rows, cols, fg, wg, acc, e_buf, pf, pg, send_a, recv_a, send_b, recv_b,
     dirg, ss, ssg,
     sem_rows, sem_cols,
-    fs_z, fr_z, fs_y, fr_y, fs_c, fr_c,
+    fs_z, fr_z, fs_y, fr_y, fs_x, fr_x, fs_c, fr_c,
     ws_z, wr_z, ws_y, wr_y,
     as_, ar, bs, br,
     ds_z, dr_z, ds_y, dr_y,
@@ -45,9 +45,12 @@
     core = lax.rem(tp, 2)
     other = 1 - core
     twin = tp + 1 - 2 * core
+    half = tp // 2
+    far = 1 - half
+    across = tp + 2 - 4 * half
     T, D = rows_v.shape
     C = cols_v.shape[1]
-    R, K = fac_ref.shape[1:]
+    R, K = fac_ref.shape[2] * 2, fac_ref.shape[3]
     k = first_v.shape[0]
     TC = 512
 
@@ -88,10 +91,10 @@
     pend = []
 
     for d in list(range(1, nz)):
-        c = rcopy(fac_ref.at[core], fg.at[core, me], fs_z.at[d], fr_z.at[d], fsdev(2 * zup(d) + y))
+        c = rcopy(fac_ref.at[core, half], fg.at[core, me, half], fs_z.at[d], fr_z.at[d], fsdev(2 * zup(d) + y))
         c.start()
         pend.append(c)
-    c = rcopy(fac_ref.at[core], fg.at[core, me], fs_y.at[0], fr_y.at[0], fsdev(mate))
+    c = rcopy(fac_ref.at[core, half], fg.at[core, me, half], fs_y.at[0], fr_y.at[0], fsdev(mate))
     c.start()
     pend.append(c)
     for m in range(2):
@@ -118,21 +121,46 @@
         i = 2 * zdn(d) + ybar
         rcopy(wg.at[i], wg.at[i], ws_y.at[d], wr_y.at[d], fsdev(mate)).wait_recv()
 
-    def to_twin(i, q):
-        c = rcopy(fg.at[core, i], fg.at[core, i], fs_c.at[q], fr_c.at[q], (me, twin))
+    def act(point):
+        for kind, d in PLAN[point]:
+            if d < nz:
+                (w_send if kind == 1 else w_forward)(d)
+        for d in range(4, nz):
+            if point == 0:
+                w_send(d)
+            if point == 5:
+                w_forward(d)
+
+    def mine(i):
+        return fg.at[core, i, half]
+
+    def to_mates(i, q):
+        for src, ssem, rsem, dev in (
+            (mine(i), fs_x.at[q], fr_x.at[q], (me, across)),
+            (mine(i), fs_c.at[0, q], fr_c.at[0, q], (me, twin)),
+        ):
+            c = rcopy(src, src, ssem, rsem, dev)
+            c.start()
+            pend.append(c)
+
+    def f_recv(sems, d, i):
+        rcopy(mine(i), mine(i), fs_z.at[0], sems.at[d], fsdev(mate)).wait_recv()
+
+    def f_recv_across(i, q):
+        r = fg.at[core, i, far]
+        rcopy(r, r, fs_x.at[q], fr_x.at[q], (me, across)).wait_recv()
+        c = rcopy(r, r, fs_c.at[1, q], fr_c.at[1, q], (me, twin))
         c.start()
         pend.append(c)
 
-    def f_recv(sems, d, i):
-        rcopy(fg.at[core, i], fg.at[core, i], fs_z.at[0], sems.at[d], fsdev(mate)).wait_recv()
-
     def f_recv_twin(i, q):
-        rcopy(fg.at[other, i], fg.at[other, i], fs_c.at[0], fr_c.at[q], (me, twin)).wait_recv()
+        for g, h in ((0, half), (1, far)):
+            r = fg.at[other, i, h]
+            rcopy(r, r, fs_c.at[g, q], fr_c.at[g, q], (me, twin)).wait_recv()
 
     def accumulate(m, d):
         p = zdn(d)
-        pair = jnp.concatenate([fg[m, 2 * p], fg[m, 2 * p + 1]], axis=0)
-        pair_t = pair.T
+        pair_t = fg[m, pl.ds(2 * p, 2)].reshape(2 * R, K).T
 
         @pl.loop(0, T // TC)
         def _(t):
@@ -146,35 +174,40 @@
             else:
                 acc[m, :, at] += prod
 
-    for d in range(nz):
+    def arrive(d):
         if d > 0:
             i = 2 * zdn(d) + y
             f_recv(fr_z, d, i)
-            c = rcopy(fg.at[core, i], fg.at[core, i], fs_y.at[d], fr_y.at[d], fsdev(mate))
-            c.start()
-            pend.append(c)
-            to_twin(i, 2 * d)
+            c = rcopy(mine(i), mine(i), fs_y.at[d], fr_y.at[d], fsdev(mate))
+            c.start()
+            pend.append(c)
+            to_mates(i, 2 * d)
         i = 2 * zdn(d) + ybar
         f_recv(fr_y, d, i)
-        to_twin(i, 2 * d + 1)
+        to_mates(i, 2 * d + 1)
+
+    def complete(d):
+        qs = ([(2 * zdn(d) + y, 2 * d)] if d else []) + [(2 * zdn(d) + ybar, 2 * d + 1)]
+        for i, q in qs:
+            f_recv_across(i, q)
         if d == 0:
-            for h in range(nz):
-                if h < len(W_HOOK) and W_HOOK[h] == 0 or h >= len(W_HOOK):
-                    w_send(h)
             loads[0].wait()
             loads[2].wait()
         accumulate(core, d)
-        if d > 0:
-            f_recv_twin(2 * zdn(d) + y, 2 * d)
-        f_recv_twin(i, 2 * d + 1)
+        for i, q in qs:
+            f_recv_twin(i, q)
         accumulate(other, d)
+
+    for d in range(nz):
+        arrive(d)
+        if d == 0:
+            act(0)
+        else:
+            complete(d - 1)
+    act(6)
+    complete(nz - 1)
     loads[1].wait()
     loads[3].wait()
-
-    def hook(v):
-        for h in range(min(nz, len(W_HOOK))):
-            if W_HOOK[h] == v:
-                w_send(h)
 
     def partial_products(m):
         @pl.loop(0, T // TC)
@@ -292,18 +325,19 @@
 
     partial_products(0)
     partial_products(1)
+    act(1)
     middle(0)
     middle(1)
-    hook(1)
+    act(2)
     moments(0, first_v, second_v, fnew_v, snew_v)
     moments(1, first_o, second_o, fnew_o, snew_o)
-    hook(2)
+    act(3)
     dir_forward(0)
     dir_forward(1)
+    act(4)
     expand(0)
     expand(1)
-    for h in range(1, nz):
-        w_forward(h)
+    act(5)
     for h in range(nz):
         w_finish(h)
     finish(0, w_v, step_v, upd_v, copy_v)
@@ -337,7 +371,7 @@
         scratch_shapes=[
             pltpu.VMEM((2, T, D), BF16),
             pltpu.VMEM((2, T, C), BF16),
-            pltpu.VMEM((2, n, R, K), BF16),
+            pltpu.VMEM((2, n, 2, R // 2, K), BF16),
             pltpu.VMEM((n, 2, R, C), BF16),
             pltpu.VMEM((2, K, T), F32),
             pltpu.VMEM((2, n, R, C), F32),
@@ -351,7 +385,7 @@
             pltpu.VMEM((2, 8, C), F32),
             pltpu.VMEM((2, ntp, 8, C), F32),
             dma((2,)), dma((2,)),
-            dma((nz,)), dma((nz,)), dma((nz,)), dma((nz,)), dma((n,)), dma((n,)),
+            dma((nz,)), dma((nz,)), dma((nz,)), dma((nz,)), dma((n,)), dma((n,)), dma((2, n)), dma((2, n)),
             dma((nz,)), dma((nz,)), dma((nz,)), dma((nz,)),
             dma((2, nz)), dma((2, nz)), dma((2, nz)), dma((2, nz)),
             dma((2, nz)), dma((2, nz)), dma((2, nz)), dma((2, nz)),
@@ -362,7 +396,7 @@
         ),
     )(
         model_input, value_cotan, mixer_cotan, head_output,
-        jnp.stack([value_factor, output_factor]),
+        jnp.stack([value_factor, output_factor]).reshape(2, 2, R // 2, K),
         value_weight, output_weight,
         value_first, output_first, value_second, output_second,
     )

time: 178 us -> 132 us (0.74)
  the two profiles are of different devices: /device:TPU:0 before, /device:TPU:17 now
where the time goes in v2:
time: 132 us
  Pallas kernels  118 us (89%)
  local copies, waits for them, and re-layouts  11.7 us (9%)
  other arithmetic  1.87 us (1%)
    pallas_call x1, Pallas kernels, local(): pl.pallas_call(functools.partial(kernel, n, ntp), out_shape=(wide, wide,...  118 us
    unnamed x24, local copies, waits for them, and re-layouts  11.7 us

profile of v2, /device:TPU:17, one launch (start us, length us, event | category | flops | bytes accessed | tf_op | source)
XLA Modules:
  0.0 132.1 jit_solution(7082239578559828523)
XLA Ops:
  0.6 1.9 %pad_maximum_fusion.fac_ref = bf16[2,2,128,512]{3,2,1,0:T(8,128)(2,1)} fusion(bf16[1,2,128,512]{3,2,1,0:T(8,128)(2,1)} %bitcast.2, bf16[1,2,128,512]{3,2,1,0:T(8,128)(2,1)} %bitcast.3), kind=kLoop, calls=%fused_computation | loop fusion | flops 262144 | bytes 1048576 | tf_op jit(solution)/shard_map/stack | solution.py:399
  2.5 117.8 %shard_map.195 = (f32[256,512]{1,0:T(8,128)}, f32[256,512]{1,0:T(8,128)}, f32[64,512]{1,0:T(8,128)}, f32[64,512]{1,0:T(8,128)}, bf16[2048,512]{1,0:T(8,128)(2,1)...) custom-call(bf16[2048,2048]{1,0:T(8,128)(2,1)} %rows_v.1, ...), custom_call_target="tpu_custom_call" | custom-call | tf_op jit(solution)/shard_map/pallas_call | solution.py:366
  120.4 0.0 copy-start.6
  120.4 0.0 copy-start.1
  120.4 2.0 %copy.32 = f32[256,512]{1,0:T(8,128)} copy(f32[256,512]{1,0:T(8,128)} %get-tuple-element.20) | data formatting | bytes 1048576
  122.4 1.9 %copy.33 = f32[256,512]{1,0:T(8,128)} copy(f32[256,512]{1,0:T(8,128)} %get-tuple-element.21) | data formatting | bytes 1048576
  124.3 1.6 %copy.34 = f32[64,512]{1,0:T(8,128)} copy(f32[64,512]{1,0:T(8,128)} %get-tuple-element.22) | data formatting | bytes 262144
  125.8 0.0 copy-done.6
  125.8 0.7 copy.35
  126.5 0.0 copy-done.1
  126.5 0.0 copy-start.3
  126.5 0.0 copy-start.2
  126.5 0.0 copy-start.5
  126.5 1.3 %copy.36 = bf16[2048,512]{1,0:T(8,128)(2,1)} copy(bf16[2048,512]{1,0:T(8,128)(2,1)S(1)} %copy-done.1) | data formatting | bytes 4194304
  127.8 0.0 copy-done.3
  127.9 0.0 copy-start.4
  127.9 0.0 copy-start
  127.9 0.8 copy.37
  128.7 0.0 copy-done.2
  128.7 0.8 copy.38
  129.5 0.0 copy-done.5
  129.5 0.7 copy.39
  130.1 0.0 copy-done.4
  130.1 0.7 copy.40
  130.8 0.0 copy-done
  130.8 1.3 copy.41
Async XLA Ops:
  120.4 5.5 %copy-start.6 = (f32[64,512]{1,0:T(8,128)S(1)}, f32[64,512]{1,0:T(8,128)}, u32[]{:S(2)}) copy-start(f32[64,512]{1,0:T(8,128)} %get-tuple-element.23) | copy-start | bytes 393220
  120.4 6.1 %copy-start.1 = (bf16[2048,512]{1,0:T(8,128)(2,1)S(1)}, bf16[2048,512]{1,0:T(8,128)(2,1)}, u32[]{:S(2)}) copy-start(bf16[2048,512]{1,0:T(8,128)(2,1)} %get-tuple-element.24) | copy-start | bytes 6291460
  126.5 1.4 %copy-start.3 = (f32[256,512]{1,0:T(8,128)S(1)}, f32[256,512]{1,0:T(8,128)}, u32[]{:S(2)}) copy-start(f32[256,512]{1,0:T(8,128)} %get-tuple-element.25) | copy-start | bytes 1572868
  126.5 2.2 %copy-start.2 = (f32[256,512]{1,0:T(8,128)S(1)}, f32[256,512]{1,0:T(8,128)}, u32[]{:S(2)}) copy-start(f32[256,512]{1,0:T(8,128)} %get-tuple-element.26) | copy-start | bytes 1572868
  126.5 3.0 %copy-start.5 = (f32[64,512]{1,0:T(8,128)S(1)}, f32[64,512]{1,0:T(8,128)}, u32[]{:S(2)}) copy-start(f32[64,512]{1,0:T(8,128)} %get-tuple-element.27) | copy-start | bytes 393220
  127.9 2.3 %copy-start.4 = (f32[64,512]{1,0:T(8,128)S(1)}, f32[64,512]{1,0:T(8,128)}, u32[]{:S(2)}) copy-start(f32[64,512]{1,0:T(8,128)} %get-tuple-element.28) | copy-start | bytes 393220
  127.9 2.9 %copy-start = (bf16[2048,512]{1,0:T(8,128)(2,1)S(1)}, bf16[2048,512]{1,0:T(8,128)(2,1)}, u32[]{:S(2)}) copy-start(bf16[2048,512]{1,0:T(8,128)(2,1)} %get-tuple-element.29) | copy-start | bytes 6291460

commit v3 on v2

--- a/solution.py
+++ b/solution.py
@@ -17,19 +17,19 @@
 F32 = jnp.float32
 BF16 = jnp.bfloat16
 VMEM_LIMIT = 67_000_000
-PLAN = (((1, 0), (1, 1), (1, 3), (1, 2)), ((2, 3),), ((2, 2),), (), (), (), ((2, 1),))
+PLAN = (((1, 0), (1, 1), (1, 3), (1, 2)), ((2, 3),), (), ((2, 2),), (), (), ((2, 1),))
 
 
 def kernel(
     n,
     ntp,
     rows_v, cols_v, rows_o, cols_o,
-    fac_ref, w_v, w_o, first_v, first_o, second_v, second_o,
+    fac_v, fac_o, w_v, w_o, first_v, first_o, second_v, second_o,
     step_v, upd_v, fnew_v, snew_v, copy_v,
     step_o, upd_o, fnew_o, snew_o, copy_o,
     rows, cols, fg, wg, acc, e_buf, pf, pg, send_a, recv_a, send_b, recv_b,
     dirg, ss, ssg,
-    sem_rows, sem_cols,
+    sem_rows, sem_cols, sem_fac,
     fs_z, fr_z, fs_y, fr_y, fs_x, fr_x, fs_c, fr_c,
     ws_z, wr_z, ws_y, wr_y,
     as_, ar, bs, br,
@@ -50,7 +50,7 @@
     across = tp + 2 - 4 * half
     T, D = rows_v.shape
     C = cols_v.shape[1]
-    R, K = fac_ref.shape[2] * 2, fac_ref.shape[3]
+    R, K = fac_v.shape[1] * 2, fac_v.shape[2]
     k = first_v.shape[0]
     TC = 512
 
@@ -73,6 +73,12 @@
     for m, (r, c) in enumerate(((rows_v, cols_v), (rows_o, cols_o))):
         loads.append(pltpu.make_async_copy(r, rows.at[m], sem_rows.at[m]))
         loads.append(pltpu.make_async_copy(c, cols.at[m], sem_cols.at[m]))
+    own = [
+        pltpu.make_async_copy(r, fg.at[m, me], sem_fac.at[m])
+        for m, r in enumerate((fac_v, fac_o))
+    ]
+    for c in own:
+        c.start()
     for i in (0, 2, 1, 3):
         loads[i].start()
 
@@ -89,16 +95,16 @@
     pl.semaphore_wait(barrier, nz - 1 + 1 + ntp - 1)
 
     pend = []
+    for c in own:
+        c.wait()
 
     for d in list(range(1, nz)):
-        c = rcopy(fac_ref.at[core, half], fg.at[core, me, half], fs_z.at[d], fr_z.at[d], fsdev(2 * zup(d) + y))
+        c = rcopy(fg.at[core, me, half], fg.at[core, me, half], fs_z.at[d], fr_z.at[d], fsdev(2 * zup(d) + y))
         c.start()
         pend.append(c)
-    c = rcopy(fac_ref.at[core, half], fg.at[core, me, half], fs_y.at[0], fr_y.at[0], fsdev(mate))
+    c = rcopy(fg.at[core, me, half], fg.at[core, me, half], fs_y.at[0], fr_y.at[0], fsdev(mate))
     c.start()
     pend.append(c)
-    for m in range(2):
-        fg[m, me] = fac_ref[m]
     wg[me, 0] = w_v[...].astype(BF16)
     wg[me, 1] = w_o[...].astype(BF16)
 
@@ -346,6 +352,20 @@
         c.wait_send()
 
 
+def deliver(count, *refs):
+    srcs, dsts, bufs = refs[:count], refs[count:2 * count], refs[2 * count:3 * count]
+    sem_in, sem_out = refs[3 * count:]
+    ins = [pltpu.make_async_copy(a, b, sem_in.at[i]) for i, (a, b) in enumerate(zip(srcs, bufs))]
+    outs = [pltpu.make_async_copy(a, b, sem_out.at[i]) for i, (a, b) in enumerate(zip(bufs, dsts))]
+    for c in ins:
+        c.start()
+    for a, b in zip(ins, outs):
+        a.wait()
+        b.start()
+    for c in outs:
+        c.wait()
+
+
 def local(
     n, ntp,
     model_input, value_cotan, mixer_cotan, head_output,
@@ -363,10 +383,10 @@
     mom = jax.ShapeDtypeStruct((k, C), F32)
     full = jax.ShapeDtypeStruct((n * R, C), BF16)
     dma = pltpu.SemaphoreType.DMA
-    return pl.pallas_call(
+    results = pl.pallas_call(
         functools.partial(kernel, n, ntp),
         out_shape=(wide, wide, mom, mom, full) * 2,
-        in_specs=[hbm] * 4 + [vm] * 7,
+        in_specs=[hbm] * 6 + [vm] * 6,
         out_specs=(vm,) * 10,
         scratch_shapes=[
             pltpu.VMEM((2, T, D), BF16),
@@ -384,7 +404,7 @@
             pltpu.VMEM((2, n, k, C), BF16),
             pltpu.VMEM((2, 8, C), F32),
             pltpu.VMEM((2, ntp, 8, C), F32),
-            dma((2,)), dma((2,)),
+            dma((2,)), dma((2,)), dma((2,)),
             dma((nz,)), dma((nz,)), dma((nz,)), dma((nz,)), dma((n,)), dma((n,)), dma((2, n)), dma((2, n)),
             dma((nz,)), dma((nz,)), dma((nz,)), dma((nz,)),
             dma((2, nz)), dma((2, nz)), dma((2, nz)), dma((2, nz)),
@@ -396,10 +416,18 @@
         ),
     )(
         model_input, value_cotan, mixer_cotan, head_output,
-        jnp.stack([value_factor, output_factor]).reshape(2, 2, R // 2, K),
+        value_factor.reshape(2, R // 2, K), output_factor.reshape(2, R // 2, K),
         value_weight, output_weight,
         value_first, output_first, value_second, output_second,
     )
+    return pl.pallas_call(
+        functools.partial(deliver, len(results)),
+        out_shape=tuple(jax.ShapeDtypeStruct(r.shape, r.dtype) for r in results),
+        in_specs=[hbm] * len(results),
+        out_specs=(hbm,) * len(results),
+        scratch_shapes=[pltpu.VMEM(r.shape, r.dtype) for r in results]
+        + [dma((len(results),)), dma((len(results),))],
+    )(*results)
 
 
 def solution(mesh):

time: 132 us -> 127 us (0.962)
  local copies, waits for them, and re-layouts: 11.7 us -> 0 us
  Pallas kernels: 118 us -> 126 us
  other arithmetic: 1.87 us -> 0 us
    unnamed x24 -> x0, local copies, waits for them, and re-layouts: 11.7 us -> none
    pallas_call x0 -> x1, Pallas kernels: none -> 6.17 us  [local(): pl.pallas_call(functools.partial(deliver, len(results)), out_shape=tuple(...]
    pallas_call x1, Pallas kernels: 118 us -> 120 us  [local(): pl.pallas_call(functools.partial(kernel, n, ntp), out_shape=(wide, wide,...]
    another operation x1 -> x0, other arithmetic: 1.87 us -> none  [local(): jnp.stack([value_factor, output_factor]).reshape(2, 2, R // 2, K)]
where the time goes in v3:
time: 127 us
  Pallas kernels  126 us (99%)
    pallas_call x1, Pallas kernels, local(): pl.pallas_call(functools.partial(kernel, n, ntp), out_shape=(wide, wide,...  120 us
    pallas_call x1, Pallas kernels, local(): pl.pallas_call(functools.partial(deliver, len(results)), out_shape=tuple(...  6.17 us

profile of v3, /device:TPU:17, one launch (start us, length us, event | category | flops | bytes accessed | tf_op | source)
XLA Modules:
  0.0 126.6 jit_solution(8321031020880721871)
XLA Ops:
  0.6 119.8 %shard_map.195 = (f32[256,512]{1,0:T(8,128)}, f32[256,512]{1,0:T(8,128)}, f32[64,512]{1,0:T(8,128)}, f32[64,512]{1,0:T(8,128)}, bf16[2048,512]{1,0:T(8,128)(2,1)...) custom-call(bf16[2048,2048]{1,0:T(8,128)(2,1)} %rows_v.1, ...), custom_call_target="tpu_custom_call" | custom-call | tf_op jit(solution)/shard_map/pallas_call | solution.py:386
  120.4 6.2 %shard_map.196 = (f32[256,512]{1,0:T(8,128)}, f32[256,512]{1,0:T(8,128)}, f32[64,512]{1,0:T(8,128)}, f32[64,512]{1,0:T(8,128)}, bf16[2048,512]{1,0:T(8,128)(2,1)...) custom-call(f32[256,512]{1,0:T(8,128)} %get-tuple-element.20.refs_0_, ...), custom_call_target="tpu_custom_call" | custom-call | tf_op jit(solution)/shard_map/pallas_call | solution.py:423
